TPU v7x, 32 devices: a whole 2x2x4 slice. The times are simulated.
32 devices in a mesh: ep: 8 (over z, y), tp: 4 (over x, core).
Axes of the slice: x: 2, y: 2, z: 4, core: 2. Of those that a mesh axis runs over, the one named last changes fastest.
Arguments:
- queries: bfloat16 [4096, 1024], P('ep', 'tp'), may hold values from -6 to 6
- keys: bfloat16 [4096, 512], P('ep', 'tp'), may hold values from -6 to 6
- values: bfloat16 [4096, 512], P('ep', 'tp'), may hold values from -6 to 6
- forget_cache: float32 [8, 4096], P('tp'), may hold values from -412 to 0, as said below
- query_gain: float32 [128], replicated, may hold values from 0.6 to 6
- key_gain: float32 [128], replicated, may hold values from 0.6 to 6
- mixer_out: bfloat16 [1024, 2048], replicated, may hold values from -0.75 to 0.75
- expert_input: bfloat16 [4096, 2048], P(('ep', 'tp')), may hold values from -6 to 6
- norm_gain: float32 [2048], replicated, may hold values from 0.1 to 1.9
- routes: int32 [4096, 2], P(('ep', 'tp')), may hold values from 0 to 31, all different within a row; in each aligned block of 128 rows (0 to 127, 128 to 255, ...) at most 16 rows name the same one
- route_weights: float32 [4096, 2], P(('ep', 'tp')), may hold values from 0.1 to 1
- w_gate: bfloat16 [32, 2048, 1024], P('ep', None, 'tp'), may hold values from -0.125 to 0.125
- w_up: bfloat16 [32, 2048, 1024], P('ep', None, 'tp'), may hold values from -0.125 to 0.125
- w_down: bfloat16 [32, 2048, 1024], P('ep', None, 'tp'), may hold values from -0.1875 to 0.1875
Outputs:
- mixed: bfloat16 [4096, 2048], P(('ep', 'tp'))
- routed: bfloat16 [4096, 2048], P(('ep', 'tp'))
Inputs may be any that keep to these rules, and one draw needn't show every extreme that they name: `routes`: each row names 2 different experts; among the rows of one device no expert is named by more than 16 rows, a bound that some block reaches. `forget_cache`: never rises along the positions.
All inputs are finite; a program needn't handle non-finite values.
Results may differ from a plain program's by a relative error of at most 0.013.
The roundings to bfloat16 on the way count: a program that leaves them out, or rounds other values in their place, can miss the bound.
Values may be sent and summed in bfloat16 or wider, within the bound.
A program may use at most 128 MiB of HBM per device.

v0:
```python
import math
import jax
import jax.numpy as jnp
from jax import lax
from jax.sharding import PartitionSpec as P

EXPERTS = 32
CAP = 16
EPSILON = 1e-06
NEGATIVE = -1e30


def rms_scale(inputs, gain):
    inputs = inputs.astype(jnp.float32)
    return inputs * lax.rsqrt(jnp.mean(inputs * inputs, axis=-1, keepdims=True) + EPSILON) * gain


def attend(queries, keys, values, forget_cache, query_gain, key_gain):
    rows = queries.shape[0]
    head_dim = keys.shape[1]
    local_heads = forget_cache.shape[0]
    first = lax.axis_index("ep") * rows
    normed_q = rms_scale(queries.reshape(rows, local_heads, head_dim), query_gain).astype(
        jnp.bfloat16
    )
    normed_k = rms_scale(keys, key_gain).astype(jnp.bfloat16)
    scale = head_dim ** (-0.5)
    groups = [(normed_q, first + jnp.arange(rows, dtype=jnp.int32))]
    gate_sets = [jnp.take(forget_cache, position, axis=1) for _, position in groups]
    initial = tuple(
        (
            (
                jnp.full((local_heads, group_rows.shape[0]), NEGATIVE, jnp.float32),
                jnp.zeros((local_heads, group_rows.shape[0]), jnp.float32),
                jnp.zeros((local_heads, group_rows.shape[0], head_dim), jnp.float32),
            )
            for group_rows, _ in groups
        )
    )
    key_matrix_rows = lax.all_gather(normed_k, "ep", axis=0, tiled=True)
    value_rows = lax.all_gather(values, "ep", axis=0, tiled=True)
    length = key_matrix_rows.shape[0]
    width = math.gcd(length, 512)
    query_rows, query_pos = groups[0]
    query_gates = gate_sets[0]
    last_pos = jnp.max(query_pos)

    def one_block(number, inner):
        begin = number * width

        def update(current):
            highest, denom, accum = current
            block_keys = lax.dynamic_slice_in_dim(key_matrix_rows, number * width, width, 0)
            block_values = lax.dynamic_slice_in_dim(value_rows, number * width, width, 0)
            key_gates = lax.dynamic_slice_in_dim(forget_cache, begin, width, 1)
            scores = (
                jnp.einsum(
                    "qhd,kd->hqk", query_rows, block_keys, preferred_element_type=jnp.float32
                )
                * scale
            )
            scores = scores + query_gates[:, :, None] - key_gates[:, None, :]
            key_pos = begin + jnp.arange(width, dtype=jnp.int32)
            allowed = key_pos[None, :] <= query_pos[:, None]
            scores = jnp.where(allowed[None], scores, NEGATIVE)
            newest = jnp.maximum(highest, jnp.max(scores, axis=2))
            weights = jnp.where(allowed[None], jnp.exp(scores - newest[:, :, None]), 0.0)
            factor = jnp.exp(highest - newest)
            denom = denom * factor + jnp.sum(weights, axis=2)
            product = jnp.einsum(
                "hqk,kd->hqd",
                weights.astype(jnp.bfloat16),
                block_values,
                preferred_element_type=jnp.float32,
            )
            accum = accum * factor[:, :, None] + product
            return (newest, denom, accum)

        return lax.cond(begin <= last_pos, update, lambda current: current, inner)

    results = [lax.fori_loop(0, length // width, one_block, initial[0])]
    finals = tuple(results)
    outputs = [(accum / denom[:, :, None]).astype(jnp.bfloat16) for _, denom, accum in finals]
    return outputs[0]


def dispatch(expert_input, norm_gain, routes):
    rows = expert_input.shape[0]
    top = routes.shape[1]
    normed = rms_scale(expert_input, norm_gain).astype(jnp.bfloat16)
    flat = routes.reshape(-1)
    onehot = (flat[:, None] == jnp.arange(EXPERTS, dtype=jnp.int32)[None, :]).astype(jnp.int32)
    prior_state = jnp.cumsum(onehot, axis=0) - onehot
    rank = jnp.sum(prior_state * onehot, axis=1)
    slots = rank * EXPERTS + flat
    owner = (
        jnp.full((CAP * EXPERTS,), rows, jnp.int32)
        .at[slots]
        .set(jnp.arange(rows * top, dtype=jnp.int32) // top)
    )
    padded = jnp.concatenate([normed, jnp.zeros((1, normed.shape[1]), jnp.bfloat16)], axis=0)
    outgoing = padded[owner].reshape(CAP, EXPERTS, normed.shape[1])
    received = lax.all_to_all(outgoing, "ep", split_axis=1, concat_axis=0, tiled=True)
    return (received, slots)


def on_device(
    queries,
    keys,
    values,
    forget_cache,
    query_gain,
    key_gain,
    mixer_out,
    expert_input,
    norm_gain,
    routes,
    route_weights,
    w_gate,
    w_up,
    w_down,
):
    attended = attend(queries, keys, values, forget_cache, query_gain, key_gain)
    received, slots = dispatch(expert_input, norm_gain, routes)
    regrouped = lax.all_to_all(attended, "tp", split_axis=1, concat_axis=0, tiled=True)
    all_heads = regrouped.shape[0]
    projection = mixer_out.reshape(all_heads, regrouped.shape[2], mixer_out.shape[1])
    mixed = jnp.einsum(
        "hqd,hde->qe", regrouped, projection, preferred_element_type=jnp.float32
    ).astype(jnp.bfloat16)
    pieces = lax.all_gather(received, "tp", axis=0, tiled=True)
    gate = jnp.einsum("red,edf->ref", pieces, w_gate, preferred_element_type=jnp.float32)
    upward = jnp.einsum("red,edf->ref", pieces, w_up, preferred_element_type=jnp.float32)
    hidden = (jax.nn.silu(gate) * upward).astype(jnp.bfloat16)
    summed = lax.psum_scatter(
        jnp.einsum("ref,edf->red", hidden, w_down, preferred_element_type=jnp.float32).astype(
            jnp.bfloat16
        ),
        "tp",
        scatter_dimension=0,
        tiled=True,
    )
    returned = lax.all_to_all(summed, "ep", split_axis=0, concat_axis=1, tiled=True)
    flat_back = returned.reshape(-1, returned.shape[2])
    picked = (
        flat_back[slots]
        .reshape(routes.shape[0], routes.shape[1], returned.shape[2])
        .astype(jnp.float32)
    )
    routed = jnp.sum(picked * route_weights[:, :, None], axis=1).astype(jnp.bfloat16)
    return (mixed, routed)


def solution(mesh):
    in_specs = (
        P("ep", "tp"),
        P("ep", "tp"),
        P("ep", "tp"),
        P("tp", None),
        P(),
        P(),
        P(),
        P(("ep", "tp"), None),
        P(),
        P(("ep", "tp"), None),
        P(("ep", "tp"), None),
        P("ep", None, "tp"),
        P("ep", None, "tp"),
        P("ep", None, "tp"),
    )
    out_specs = (P(("ep", "tp"), None), P(("ep", "tp"), None))
    return jax.shard_map(
        on_device, mesh=mesh, in_specs=in_specs, out_specs=out_specs, check_vma=False
    )
```

profile of v0, /device:TPU:0, one launch (start us, length us, event | category | flops | bytes accessed | tf_op | source)
XLA Modules:
  0.0 367.3 jit_solution(14982361686460898123)
XLA Ops:
  7.2 0.8 copy.60
  9.4 1.4 scatter_custom_fusion
  10.8 1.2 fusion.22
  12.1 1.2 fusion.24
  13.4 2.5 gather_fusion.1
  15.8 1.2 copy.64
  17.0 55.3 %all_to_all.51 = bf16[16,32,2048]{2,0,1:T(8,128)(2,1)S(1)} all-to-all(bf16[16,32,2048]{2,0,1:T(8,128)(2,1)S(1)} %copy.64), channel_id=1, replica_groups=mesh['ep'=8,'tp'=4] {'ep'}, dimensions={1} | all-to-all | bytes 4194304 | tf_op jit(solution)/shard_map/all_to_all | solution.py:103
  72.3 1.5 copy.65
  73.9 0.8 copy-done
  74.9 0.8 fusion.30
  76.7 54.6 %all-gather.8.cloned.1.call-done = bf16[512,4,2048]{2,0,1:T(8,128)(2,1)} async-done(((bf16[128,4,2048]{2,0,1:T(8,128)(2,1)}), bf16[512,4,2048]{2,0,1:T(8,128)(2,1)}) %all-gather.8.cloned.1.call-update) | async-done | bytes 8388624 | tf_op jit(solution)/shard_map/all_gather | solution.py:131
  131.3 6.9 %fusion.42 = f32[4,512,256]{2,1,0:T(8,128)S(1)} fusion(bf16[512,4,2048]{2,0,1:T(8,128)(2,1)} %all-gather.8.cloned.1.call-done, bf16[4,2048,256]{2,1,0:T(8,128)(2,1)} %param.29), kind=kOutput, calls=%fused_computation.89 | convolution fusion | flops 2147483648 | bytes 14680064 | tf_op jit(solution)/shard_map/red,edf->ref/dot_general | solution.py:132
  138.2 14.0 %convert_bitcast_fusion = bf16[512,4,2048]{2,0,1:T(8,128)(2,1)} fusion(bf16[4,2048,256]{2,1,0:T(8,128)(2,1)} %param.31, f32[4,512,256]{2,1,0:T(8,128)S(1)} %fusion.42, bf16[512,4,2048]{2,0,1:T(8,128)(2,1)} %all-gather.8.cloned.1.call-done, bf16[4,2048,256]{2,1,0:T(8,128)(2,1)} %param.30), kind=kOutput, calls=%fused_computation.28 | convolution fusion | flops 4302307328 | bytes 27262976 | tf_op jit(solution)/shard_map/ref,edf->red/dot_general | solution.py:136
  154.2 1.0 gather_fusion
  156.1 18.2 %all-gather.4.cloned.1.call-done = bf16[4096,128]{1,0:T(8,128)(2,1)} async-done(((bf16[512,128]{1,0:T(8,128)(2,1)}), bf16[4096,128]{1,0:T(8,128)(2,1)}) %all-gather.4.cloned.1.call-update) | async-done | bytes 1048592 | tf_op jit(solution)/shard_map/all_gather | solution.py:40
  174.3 41.2 %all-gather.6.cloned.1.call-done = bf16[4096,128]{1,0:T(8,128)(2,1)} async-done(((bf16[512,128]{1,0:T(8,128)(2,1)}), bf16[4096,128]{1,0:T(8,128)(2,1)}) %all-gather.6.cloned.1.call-update) | async-done | bytes 1048592 | tf_op jit(solution)/shard_map/all_gather | solution.py:41
  215.5 8.8 %while.18 = (s32[]{:T(128)}, f32[2,512]{1,0:T(2,128)S(1)}, f32[2,512]{1,0:T(2,128)S(1)}, f32[2,512,128]{2,1,0:T(8,128)S(1)}, s32[]{:T(128)}, /*index=5*/bf16[409...) while((s32[]{:T(128)}, f32[2,512]{1,0:T(2,128)S(1)}, ...), condition=%wide.region_8.9_spmd.clone, body=%wide.region_3.8_spmd.clone.sunk | while | flops 274729984 | bytes 9007507 | solution.py:81
  216.1 4.0 %conditional.3 = ((f32[2,512]{1,0:T(2,128)S(1)}, f32[2,512]{1,0:T(2,128)S(1)}, f32[2,512,128]{2,1,0:T(8,128)S(1)})) conditional(s32[]{:T(128)} %convert_element_type.114, (f32[2,512]{1,0:T(2,128)S(1)}, f32[2,512]{1,0:T(2,128)S(1)}, f32[2,512,128]{2,1,0:T(8,128)S(1)}) %tuple.53, (s32[]{:T(128)}, s32[]{:T(128)}, s32[]{:T(128)}, ...), branch_computations={%region_4.4_spmd, %region_5.0_spmd} | conditional | flops 274729984 | bytes 9005188 | solution.py:79
  216.4 1.6 fusion.41
  218.4 1.7 convolution_add_fusion
  224.5 1.0 copy.58
  225.5 3.6 all-to-all-start
  229.1 58.9 %reduce-scatter.2.cloned.1.call-done = bf16[128,4,2048]{2,0,1:T(8,128)(2,1)} async-done(((bf16[512,4,2048]{2,0,1:T(8,128)(2,1)}), bf16[128,4,2048]{2,0,1:T(8,128)(2,1)}) %reduce-scatter.2.cloned.1.call-update) | async-done | bytes 2097168 | tf_op jit(solution)/shard_map/reduce_scatter | solution.py:135
  288.0 4.6 %copy.66 = bf16[128,4,2048]{2,1,0:T(4,128)(2,1)} copy(bf16[128,4,2048]{2,0,1:T(8,128)(2,1)} %reduce-scatter.2.cloned.1.call-done) | data formatting | bytes 4194304 | tf_op jit(solution)/shard_map/reduce_scatter | solution.py:135
  292.6 8.5 %all-to-all-start.2 = ((bf16[128,4,2048]{2,1,0:T(4,128)(2,1)}), bf16[128,4,2048]{2,1,0:T(4,128)(2,1)S(1)}, u32[]{:S(2)}, u32[]{:S(2)}) async-start(bf16[128,4,2048]{2,1,0:T(4,128)(2,1)} %copy.66), calls=%async_computation.3 | async-start | bytes 4194304 | tf_op jit(solution)/shard_map/all_to_all | solution.py:143
  301.2 3.7 %fusion.17 = bf16[128,2048]{1,0:T(8,128)(2,1)} fusion(bf16[8,128,128]{2,1,0:T(8,128)(2,1)S(1)} %bitcast.110, bf16[8,128,2048]{2,1,0:T(8,128)(2,1)} %bitcast.109), kind=kOutput, calls=%fused_computation.30 | convolution fusion | flops 537133056 | bytes 4980736 | tf_op jit(solution)/shard_map/hqd,hde->qe/dot_general | solution.py:128
  304.9 44.2 %all-to-all-done.2 = bf16[128,4,2048]{2,1,0:T(4,128)(2,1)S(1)} async-done(((bf16[128,4,2048]{2,1,0:T(4,128)(2,1)}), bf16[128,4,2048]{2,1,0:T(4,128)(2,1)S(1)}, u32[]{:S(2)}, u32[]{:S(2)}) %all-to-all-start.2) | async-done | bytes 2097184 | tf_op jit(solution)/shard_map/all_to_all | solution.py:143
  349.1 2.4 copy.73
  351.5 2.5 reshape.156
  354.0 1.4 gather_fusion.2
  355.4 1.3 reshape.158
  356.7 4.0 %multiply_reduce_fusion = bf16[128,2048]{1,0:T(8,128)(2,1)} fusion(f32[128,2,2048]{2,1,0:T(2,128)S(1)} %reshape.158, f32[128,2]{1,0:T(8,128)S(1)} %copy.68), kind=kLoop, calls=%fused_computation.39 | loop fusion | flops 786432 | bytes 2622464 | tf_op jit(solution)/shard_map/reduce_sum | solution.py:150
  (79 shorter events, 6.6 us)
Async XLA Ops:
  7.2 124.1 %all-gather.8.cloned.1.call-start = ((), (), s32[]{:S(2)}) async-start(), calls=%async_computation.6 | async-start | bytes 10485760 | tf_op jit(solution)/shard_map/all_gather | solution.py:131
  73.8 0.9 copy-start
  73.8 1.1 copy-start.4
  73.8 100.4 %all-gather.4.cloned.1.call-start = ((), (), s32[]{:S(2)}) async-start(), calls=%async_computation.4 | async-start | bytes 1179648 | tf_op jit(solution)/shard_map/all_gather | solution.py:40
  75.7 139.7 %all-gather.6.cloned.1.call-start = ((), (), s32[]{:S(2)}) async-start(), calls=%async_computation.5 | async-start | bytes 1179648 | tf_op jit(solution)/shard_map/all_gather | solution.py:41
  76.5 211.6 %reduce-scatter.2.cloned.1.call-start = ((), (), s32[]{:S(2)}) async-start(), calls=%async_computation.7 | async-start | bytes 10485760 | tf_op jit(solution)/shard_map/reduce_scatter | solution.py:135
  152.2 0.8 copy-start.2
  152.2 3.3 copy-start.1
  152.2 3.6 copy-start.5
  225.5 67.1 %all-to-all-start = ((bf16[2,512,128]{2,0,1:T(2,128)(2,1)}), bf16[2,512,128]{2,0,1:T(2,128)(2,1)S(1)}, u32[]{:S(2)}, u32[]{:S(2)}) async-start(bf16[2,512,128]{2,0,1:T(2,128)(2,1)} %copy.58), calls=%async_computation | async-start | bytes 524288 | tf_op jit(solution)/shard_map/all_to_all | solution.py:125
  292.6 8.5 %copy-start.3 = (f32[128,2]{0,1:T(2,128)S(1)}, f32[128,2]{0,1:T(2,128)}, u32[]{:S(2)}) copy-start(f32[128,2]{0,1:T(2,128)} %param.28) | copy-start | bytes 3076
  292.6 56.5 %all-to-all-start.2 = ((bf16[128,4,2048]{2,1,0:T(4,128)(2,1)}), bf16[128,4,2048]{2,1,0:T(4,128)(2,1)S(1)}, u32[]{:S(2)}, u32[]{:S(2)}) async-start(bf16[128,4,2048]{2,1,0:T(4,128)(2,1)} %copy.66), calls=%async_computation.3 | async-start | bytes 4194304 | tf_op jit(solution)/shard_map/all_to_all | solution.py:143
Sparse Core Ops, SparseCore 0:
  74.0 57.2 all-gather.7
  134.0 40.2 all-gather.3
  176.4 38.9 all-gather.5
  217.9 70.0 reduce-scatter.1
where the time goes:
time: 368 us; the launch traced here: 367 us
  waiting for transfers between devices  218 us (59%)
  blocking collectives  55.3 us (15%)
  matrix products  27.9 us (8%)
  local copies, waits for them, and re-layouts  25 us (7%)
  between operations  14 us (4%)
  starting transfers between devices  12.5 us (3%)
  other arithmetic  10.1 us (3%)
  loops' own time  4.82 us (1%)
    reduce_scatter x1, waiting for transfers between devices, on_device(): lax.psum_scatter(jnp.einsum('ref,edf->red', hidden, w_down, preferred_ele...  58.9 us
    all_to_all x1, blocking collectives, dispatch(): lax.all_to_all(outgoing, 'ep', split_axis=1, concat_axis=0, tiled=True)  55.3 us
    all_gather x1, waiting for transfers between devices, on_device(): pieces = lax.all_gather(received, 'tp', axis=0, tiled=True)  54.6 us
    all_to_all x1, waiting for transfers between devices, on_device(): lax.all_to_all(summed, 'ep', split_axis=0, concat_axis=1, tiled=True)  44.2 us
    all_gather x1, waiting for transfers between devices, attend(): value_rows = lax.all_gather(values, 'ep', axis=0, tiled=True)  41.2 us
    all_gather x1, waiting for transfers between devices, attend(): key_matrix_rows = lax.all_gather(normed_k, 'ep', axis=0, tiled=True)  18.2 us
    dot_general x1, matrix products, on_device(): jnp.einsum('ref,edf->red', hidden, w_down, preferred_element_type=jnp.flo...  14 us
    all_to_all x1, starting transfers between devices, on_device(): lax.all_to_all(summed, 'ep', split_axis=0, concat_axis=1, tiled=True)  8.48 us
  transfers between devices with their start and end apart: 6, of which 5 were waited for; matrix products, arithmetic and copies ran while one was open for 10% of the time, Pallas kernels for 0%

commit v1 on v0

--- a/solution.py
+++ b/solution.py
@@ -140,7 +140,10 @@
         scatter_dimension=0,
         tiled=True,
     )
-    returned = lax.all_to_all(summed, "ep", split_axis=0, concat_axis=1, tiled=True)
+    returned = jnp.concatenate(
+        lax.all_to_all(jnp.stack(jnp.split(summed, lax.axis_size("ep"), axis=0)), "ep", 0, 0),
+        axis=1,
+    )
     flat_back = returned.reshape(-1, returned.shape[2])
     picked = (
         flat_back[slots]

time: 368 us -> 373 us (1.014)
  local copies, waits for them, and re-layouts: 25 us -> 30.1 us
    unnamed x18 -> x27, local copies, waits for them, and re-layouts: 3.55 us -> 11.7 us
    reduce_scatter x1 -> x0, local copies, waits for them, and re-layouts: 4.56 us -> none  [on_device(): lax.psum_scatter(jnp.einsum('ref,edf->red', hidden, w_down, preferred_ele...]
  transfers between devices with their start and end apart: 6 -> 6, of which waited for: 5 -> 5; matrix products, arithmetic and copies ran while one was open for 10% -> 11% of each run, Pallas kernels for 0% -> 0%
where the time goes in v1:
time: 373 us; the launch traced here: 372 us
  waiting for transfers between devices  218 us (58%)
  blocking collectives  55.3 us (15%)
  local copies, waits for them, and re-layouts  30.1 us (8%)
  matrix products  27.8 us (7%)
  between operations  14.1 us (4%)
  starting transfers between devices  12.2 us (3%)
  other arithmetic  9.95 us (3%)
  loops' own time  4.82 us (1%)
    reduce_scatter x1, waiting for transfers between devices, on_device(): lax.psum_scatter(jnp.einsum('ref,edf->red', hidden, w_down, preferred_ele...  59.1 us
    all_to_all x1, blocking collectives, dispatch(): lax.all_to_all(outgoing, 'ep', split_axis=1, concat_axis=0, tiled=True)  55.3 us
    all_gather x1, waiting for transfers between devices, on_device(): pieces = lax.all_gather(received, 'tp', axis=0, tiled=True)  54.6 us
    all_to_all x1, waiting for transfers between devices, on_device(): lax.all_to_all(jnp.stack(jnp.split(summed, lax.axis_size('ep'), axis=0)),...  44.2 us
    all_gather x1, waiting for transfers between devices, attend(): value_rows = lax.all_gather(values, 'ep', axis=0, tiled=True)  41.2 us
    all_gather x1, waiting for transfers between devices, attend(): key_matrix_rows = lax.all_gather(normed_k, 'ep', axis=0, tiled=True)  18.3 us
    dot_general x1, matrix products, on_device(): jnp.einsum('ref,edf->red', hidden, w_down, preferred_element_type=jnp.flo...  13.9 us
    unnamed x27, local copies, waits for them, and re-layouts  11.7 us
  transfers between devices with their start and end apart: 6, of which 5 were waited for; matrix products, arithmetic and copies ran while one was open for 11% of the time, Pallas kernels for 0%

profile of v1, /device:TPU:0, one launch (start us, length us, event | category | flops | bytes accessed | tf_op | source)
XLA Modules:
  0.0 372.4 jit_solution(14994282255550130991)
XLA Ops:
  9.4 1.4 scatter_custom_fusion
  10.8 1.2 fusion.22
  12.1 1.2 fusion.24
  13.4 2.5 gather_fusion.1
  15.8 1.2 copy.62
  17.0 55.3 %all_to_all.41 = bf16[16,32,2048]{2,0,1:T(8,128)(2,1)S(1)} all-to-all(bf16[16,32,2048]{2,0,1:T(8,128)(2,1)S(1)} %copy.62), channel_id=1, replica_groups=mesh['ep'=8,'tp'=4] {'ep'}, dimensions={1} | all-to-all | bytes 4194304 | tf_op jit(solution)/shard_map/all_to_all | solution.py:103
  72.3 1.5 copy.63
  76.7 54.6 %all-gather.8.cloned.1.call-done = bf16[512,4,2048]{2,0,1:T(8,128)(2,1)} async-done(((bf16[128,4,2048]{2,0,1:T(8,128)(2,1)}), bf16[512,4,2048]{2,0,1:T(8,128)(2,1)}) %all-gather.8.cloned.1.call-update) | async-done | bytes 8388624 | tf_op jit(solution)/shard_map/all_gather | solution.py:131
  131.3 6.9 %fusion.50 = f32[4,512,256]{2,1,0:T(8,128)S(1)} fusion(bf16[512,4,2048]{2,0,1:T(8,128)(2,1)} %all-gather.8.cloned.1.call-done, bf16[4,2048,256]{2,1,0:T(8,128)(2,1)} %param.29), kind=kOutput, calls=%fused_computation.104 | convolution fusion | flops 2147483648 | bytes 14680064 | tf_op jit(solution)/shard_map/red,edf->ref/dot_general | solution.py:132
  138.2 13.9 %convert_bitcast_fusion = bf16[512,4,2048]{2,0,1:T(8,128)(2,1)} fusion(bf16[4,2048,256]{2,1,0:T(8,128)(2,1)} %param.31, f32[4,512,256]{2,1,0:T(8,128)S(1)} %fusion.50, bf16[512,4,2048]{2,0,1:T(8,128)(2,1)} %all-gather.8.cloned.1.call-done, bf16[4,2048,256]{2,1,0:T(8,128)(2,1)} %param.30), kind=kOutput, calls=%fused_computation.28 | convolution fusion | flops 4302307328 | bytes 27262976 | tf_op jit(solution)/shard_map/ref,edf->red/dot_general | solution.py:136
  154.1 1.0 gather_fusion
  156.0 18.3 %all-gather.4.cloned.1.call-done = bf16[4096,128]{1,0:T(8,128)(2,1)} async-done(((bf16[512,128]{1,0:T(8,128)(2,1)}), bf16[4096,128]{1,0:T(8,128)(2,1)}) %all-gather.4.cloned.1.call-update) | async-done | bytes 1048592 | tf_op jit(solution)/shard_map/all_gather | solution.py:40
  174.3 41.2 %all-gather.6.cloned.1.call-done = bf16[4096,128]{1,0:T(8,128)(2,1)} async-done(((bf16[512,128]{1,0:T(8,128)(2,1)}), bf16[4096,128]{1,0:T(8,128)(2,1)}) %all-gather.6.cloned.1.call-update) | async-done | bytes 1048592 | tf_op jit(solution)/shard_map/all_gather | solution.py:41
  215.5 8.8 %while.18 = (s32[]{:T(128)}, f32[2,512]{1,0:T(2,128)S(1)}, f32[2,512]{1,0:T(2,128)S(1)}, f32[2,512,128]{2,1,0:T(8,128)S(1)}, s32[]{:T(128)}, /*index=5*/bf16[409...) while((s32[]{:T(128)}, f32[2,512]{1,0:T(2,128)S(1)}, ...), condition=%wide.region_8.9_spmd.clone, body=%wide.region_3.8_spmd.clone.sunk | while | flops 274729984 | bytes 9007507 | solution.py:81
  216.1 4.1 %conditional.3 = ((f32[2,512]{1,0:T(2,128)S(1)}, f32[2,512]{1,0:T(2,128)S(1)}, f32[2,512,128]{2,1,0:T(8,128)S(1)})) conditional(s32[]{:T(128)} %convert_element_type.114, (f32[2,512]{1,0:T(2,128)S(1)}, f32[2,512]{1,0:T(2,128)S(1)}, f32[2,512,128]{2,1,0:T(8,128)S(1)}) %tuple.54, (s32[]{:T(128)}, s32[]{:T(128)}, s32[]{:T(128)}, ...), branch_computations={%region_4.4_spmd, %region_5.0_spmd} | conditional | flops 274729984 | bytes 9005188 | solution.py:79
  216.4 1.6 fusion.49
  218.4 1.7 convolution_add_fusion
  225.5 3.4 all-to-all-start
  229.0 59.1 %reduce-scatter.2.cloned.1.call-done = bf16[128,4,2048]{2,0,1:T(8,128)(2,1)} async-done(((bf16[512,4,2048]{2,0,1:T(8,128)(2,1)}), bf16[128,4,2048]{2,0,1:T(8,128)(2,1)}) %reduce-scatter.2.cloned.1.call-update) | async-done | bytes 2097168 | tf_op jit(solution)/shard_map/reduce_scatter | solution.py:135
  289.0 1.0 fusion.37
  290.0 1.0 fusion.36
  290.9 1.0 fusion.35
  291.9 1.0 fusion.34
  295.8 1.3 copy-done
  297.2 8.5 %all-to-all-start.2 = ((bf16[8,16,4,2048]{3,1,2,0:T(8,128)(2,1)}), bf16[8,16,4,2048]{3,1,2,0:T(8,128)(2,1)S(1)}, u32[]{:S(2)}, u32[]{:S(2)}) async-start(bf16[8,16,4,2048]{3,1,2,0:T(8,128)(2,1)} %copy-done), calls=%async_computation.3 | async-start | bytes 4194304 | tf_op jit(solution)/shard_map/all_to_all | solution.py:144
  305.8 3.7 %fusion.17 = bf16[128,2048]{1,0:T(8,128)(2,1)} fusion(bf16[8,128,128]{2,1,0:T(8,128)(2,1)S(1)} %bitcast.138, bf16[8,128,2048]{2,1,0:T(8,128)(2,1)} %bitcast.137), kind=kOutput, calls=%fused_computation.30 | convolution fusion | flops 537133056 | bytes 4980736 | tf_op jit(solution)/shard_map/hqd,hde->qe/dot_general | solution.py:128
  309.6 44.2 %all-to-all-done.2 = bf16[8,16,4,2048]{3,1,2,0:T(8,128)(2,1)S(1)} async-done(((bf16[8,16,4,2048]{3,1,2,0:T(8,128)(2,1)}), bf16[8,16,4,2048]{3,1,2,0:T(8,128)(2,1)S(1)}, u32[]{:S(2)}, u32[]{:S(2)}) %all-to-all-start.2) | async-done | bytes 2097184 | tf_op jit(solution)/shard_map/all_to_all | solution.py:144
  353.7 3.0 copy.64
  356.7 2.5 reshape_reshape.3
  359.2 1.4 gather_fusion.2
  360.6 1.3 reshape.157
  361.9 3.9 %multiply_reduce_fusion = bf16[128,2048]{1,0:T(8,128)(2,1)} fusion(f32[128,2,2048]{2,1,0:T(2,128)S(1)} %reshape.157, f32[128,2]{1,0:T(8,128)S(1)} %copy.65), kind=kLoop, calls=%fused_computation.38 | loop fusion | flops 786432 | bytes 2622464 | tf_op jit(solution)/shard_map/reduce_sum | solution.py:153
  (87 shorter events, 13.9 us)
Async XLA Ops:
  7.2 124.1 %all-gather.8.cloned.1.call-start = ((), (), s32[]{:S(2)}) async-start(), calls=%async_computation.6 | async-start | bytes 10485760 | tf_op jit(solution)/shard_map/all_gather | solution.py:131
  73.8 0.9 copy-start.1
  73.8 1.1 copy-start.5
  73.8 100.4 %all-gather.4.cloned.1.call-start = ((), (), s32[]{:S(2)}) async-start(), calls=%async_computation.4 | async-start | bytes 1179648 | tf_op jit(solution)/shard_map/all_gather | solution.py:40
  75.7 139.7 %all-gather.6.cloned.1.call-start = ((), (), s32[]{:S(2)}) async-start(), calls=%async_computation.5 | async-start | bytes 1179648 | tf_op jit(solution)/shard_map/all_gather | solution.py:41
  76.4 211.6 %reduce-scatter.2.cloned.1.call-start = ((), (), s32[]{:S(2)}) async-start(), calls=%async_computation.7 | async-start | bytes 10485760 | tf_op jit(solution)/shard_map/reduce_scatter | solution.py:135
  152.1 0.8 copy-start.3
  152.1 3.3 copy-start.2
  152.1 3.6 copy-start.6
  225.5 71.7 %all-to-all-start = ((bf16[2,512,128]{2,0,1:T(2,128)(2,1)}), bf16[2,512,128]{2,0,1:T(2,128)(2,1)S(1)}, u32[]{:S(2)}, u32[]{:S(2)}) async-start(bf16[2,512,128]{2,0,1:T(2,128)(2,1)} %copy.56), calls=%async_computation | async-start | bytes 524288 | tf_op jit(solution)/shard_map/all_to_all | solution.py:125
  295.8 1.4 copy-start
  297.2 8.5 %copy-start.4 = (f32[128,2]{0,1:T(2,128)S(1)}, f32[128,2]{0,1:T(2,128)}, u32[]{:S(2)}) copy-start(f32[128,2]{0,1:T(2,128)} %param.28) | copy-start | bytes 3076
  297.2 56.5 %all-to-all-start.2 = ((bf16[8,16,4,2048]{3,1,2,0:T(8,128)(2,1)}), bf16[8,16,4,2048]{3,1,2,0:T(8,128)(2,1)S(1)}, u32[]{:S(2)}, u32[]{:S(2)}) async-start(bf16[8,16,4,2048]{3,1,2,0:T(8,128)(2,1)} %copy-done), calls=%async_computation.3 | async-start | bytes 4194304 | tf_op jit(solution)/shard_map/all_to_all | solution.py:144
Sparse Core Ops, SparseCore 0:
  74.0 57.2 all-gather.7
  134.0 40.2 all-gather.3
  176.4 38.9 all-gather.5
  217.9 70.0 reduce-scatter.1
